TPU v7x, 32 devices: a whole 2x2x4 slice. The times are simulated.
32 devices in a mesh: fs: 8 (over z, y), tp: 4 (over x, core).
Axes of the slice: x: 2, y: 2, z: 4, core: 2. Of those that a mesh axis runs over, the one named last changes fastest.
Arguments:
- tokens: bfloat16 [8192, 2048], P('fs'), may hold values from -6 to 6
- norm_gain: float32 [2048], replicated, may hold values from 0.1 to 1.9
- gate_weight: bfloat16 [2048, 5632], P('fs', 'tp'), may hold values from -0.125 to 0.125
- up_weight: bfloat16 [2048, 5632], P('fs', 'tp'), may hold values from -0.125 to 0.125
- down_weight: bfloat16 [5632, 2048], P('tp', 'fs'), may hold values from -0.078125 to 0.078125
Outputs:
- mixed: bfloat16 [8192, 2048], P(('fs', 'tp'))
All inputs are finite; a program needn't handle non-finite values.
Results may differ from a plain program's by a relative error of at most 0.014.
Values may be sent and summed in bfloat16 or wider, within the bound.
A program may use at most 128 MiB of HBM per device.

v0:
```python
import jax
import jax.numpy as jnp
from jax import lax
from jax.sharding import PartitionSpec as P


def add_rows(normed, piece):
    return jnp.dot(normed, piece, preferred_element_type=jnp.float32)


def per_device(tokens, norm_gain, gate_weight, up_weight, down_weight):
    xf = tokens.astype(jnp.float32)
    scale = lax.rsqrt(jnp.mean(xf * xf, axis=-1, keepdims=True) + 1e-06)
    normed = (xf * scale * norm_gain).astype(jnp.bfloat16)

    def add_one(piece):
        return add_rows(normed, piece)

    gate = add_one(lax.all_gather(gate_weight, "fs", axis=0, tiled=True))
    up = add_one(lax.all_gather(up_weight, "fs", axis=0, tiled=True))
    hidden = (jax.nn.silu(gate) * up).astype(jnp.bfloat16)
    terms = jnp.dot(
        hidden,
        lax.all_gather(down_weight, "fs", axis=1, tiled=True),
        preferred_element_type=jnp.float32,
    )
    mixed = lax.psum_scatter(terms.astype(jnp.bfloat16), "tp", scatter_dimension=0, tiled=True)
    return mixed


def solution(mesh):
    placed = (P("fs", None), P(), P("fs", "tp"), P("fs", "tp"), P("tp", "fs"))
    return jax.shard_map(
        per_device, mesh=mesh, in_specs=placed, out_specs=P(("fs", "tp"), None), check_vma=False
    )
```

profile of v0, /device:TPU:0, one launch (start us, length us, event | category | flops | bytes accessed | tf_op | source)
XLA Modules:
  0.0 361.0 jit_solution(8216590294000677282)
XLA Ops:
  6.5 0.0 copy-start
  6.5 0.0 all-gather.4.cloned.1.call-start
  6.5 0.7 all-gather.4.cloned.1.call-update
  7.3 0.0 all-gather.6.cloned.1.call-start
  7.3 0.7 all-gather.6.cloned.1.call-update
  8.0 0.0 all-gather.8.cloned.1.call-start
  8.1 0.7 all-gather.8.cloned.1.call-update
  8.7 0.0 reduce-scatter.2.cloned.1.call-start
  8.8 3.1 fusion
  11.9 92.7 %all-gather.4.cloned.1.call-done = bf16[2048,1408]{1,0:T(8,128)(2,1)} async-done(((bf16[256,1408]{1,0:T(8,128)(2,1)}), bf16[2048,1408]{1,0:T(8,128)(2,1)}) %all-gather.4.cloned.1.call-update) | async-done | bytes 5767184 | tf_op jit(solution)/shard_map/all_gather | solution.py:19
  104.6 0.0 copy-done
  104.6 11.9 %fusion.4 = f32[1024,1408]{1,0:T(8,128)} fusion(bf16[2048,1408]{1,0:T(8,128)(2,1)} %all-gather.4.cloned.1.call-done, bf16[1024,2048]{1,0:T(8,128)(2,1)} %param.5, f32[2048]{0:T(1024)S(1)} %copy-done, f32[1024]{0:T(1024)S(1)} %add_rsqrt_fusion), kind=kOutput, calls=%fused_computation.7 | convolution fusion | flops 5913968640 | bytes 15740928 | tf_op jit(solution)/shard_map/dot_general | solution.py:8
  116.5 80.8 %all-gather.6.cloned.1.call-done = bf16[2048,1408]{1,0:T(8,128)(2,1)} async-done(((bf16[256,1408]{1,0:T(8,128)(2,1)}), bf16[2048,1408]{1,0:T(8,128)(2,1)}) %all-gather.6.cloned.1.call-update) | async-done | bytes 5767184 | tf_op jit(solution)/shard_map/all_gather | solution.py:20
  197.3 93.4 %all-gather.8.cloned.1.call-done = bf16[1408,2048]{1,0:T(8,128)(2,1)} async-done(((bf16[1408,256]{1,0:T(8,128)(2,1)}), bf16[1408,2048]{1,0:T(8,128)(2,1)}) %all-gather.8.cloned.1.call-update) | async-done | bytes 5767184 | tf_op jit(solution)/shard_map/all_gather | solution.py:24
  290.7 20.9 %convolution_convert_fusion = bf16[1024,2048]{1,0:T(8,128)(2,1)} fusion(bf16[1408,2048]{1,0:T(8,128)(2,1)} %all-gather.8.cloned.1.call-done, f32[1024,1408]{1,0:T(8,128)} %fusion.4, bf16[2048,1408]{1,0:T(8,128)(2,1)} %all-gather.6.cloned.1.call-done, bf16[1024,2048]{1,0:T(8,128)(2,1)} %param.5, f32[2048]{0:T(1024)S(1)} %copy-done, f32[1024]{0:T(1024)S(1)} %add_rsqrt_fusion), kind=kOutput, calls=%fused_computation.6 | convolution fusion | flops 11830296576 | bytes 25702400 | tf_op jit(solution)/shard_map/dot_general | solution.py:22
  311.5 0.0 reduce-scatter.2.cloned.1.call-update
  311.6 42.9 %reduce-scatter.2.cloned.1.call-done = bf16[256,2048]{1,0:T(8,128)(2,1)} async-done(((bf16[1024,2048]{1,0:T(8,128)(2,1)}), bf16[256,2048]{1,0:T(8,128)(2,1)}) %reduce-scatter.2.cloned.1.call-update) | async-done | bytes 1048592 | tf_op jit(solution)/shard_map/reduce_scatter | solution.py:27
  (1 shorter events, 0.0 us)
Async XLA Ops:
  6.5 98.1 %copy-start = (f32[2048]{0:T(1024)S(1)}, f32[2048]{0:T(1024)}, u32[]{:S(2)}) copy-start(f32[2048]{0:T(1024)} %param.6) | copy-start | bytes 24580
  6.5 98.0 %all-gather.4.cloned.1.call-start = ((), (), s32[]{:S(2)}) async-start(), calls=%async_computation.1 | async-start | bytes 6488064 | tf_op jit(solution)/shard_map/all_gather | solution.py:19
  7.3 190.0 %all-gather.6.cloned.1.call-start = ((), (), s32[]{:S(2)}) async-start(), calls=%async_computation.2 | async-start | bytes 6488064 | tf_op jit(solution)/shard_map/all_gather | solution.py:20
  8.0 282.7 %all-gather.8.cloned.1.call-start = ((), (), s32[]{:S(2)}) async-start(), calls=%async_computation.3 | async-start | bytes 6488064 | tf_op jit(solution)/shard_map/all_gather | solution.py:24
  8.7 345.7 %reduce-scatter.2.cloned.1.call-start = ((), (), s32[]{:S(2)}) async-start(), calls=%async_computation.4 | async-start | bytes 5242880 | tf_op jit(solution)/shard_map/reduce_scatter | solution.py:27
Sparse Core Ops, SparseCore 0:
  9.5 95.0 all-gather.3
  106.8 90.4 all-gather.5
  199.3 91.2 all-gather.7
  311.7 42.7 reduce-scatter.1
where the time goes:
time: 361 us
  waiting for transfers between devices  312 us (86%)
  matrix products  32.7 us (9%)
  between operations  13.1 us (4%)
    all_gather x1, waiting for transfers between devices, per_device(): lax.all_gather(down_weight, 'fs', axis=1, tiled=True)  93.4 us
    all_gather x1, waiting for transfers between devices, per_device(): gate = add_one(lax.all_gather(gate_weight, 'fs', axis=0, tiled=True))  92.7 us
    all_gather x1, waiting for transfers between devices, per_device(): up = add_one(lax.all_gather(up_weight, 'fs', axis=0, tiled=True))  80.8 us
    reduce_scatter x1, waiting for transfers between devices, per_device(): lax.psum_scatter(terms.astype(jnp.bfloat16), 'tp', scatter_dimension=0, t...  42.9 us
    dot_general x1, matrix products, per_device(): jnp.dot(hidden, lax.all_gather(down_weight, 'fs', axis=1, tiled=True), pr...  20.9 us
    dot_general x1, matrix products, add_rows(): return jnp.dot(normed, piece, preferred_element_type=jnp.float32)  11.9 us
  transfers between devices with their start and end apart: 4, of which 4 were waited for; matrix products, arithmetic and copies ran while one was open for 4% of the time, Pallas kernels for 0%

commit v1 on v0

v1 whole, which is shorter than its diff:
```python
import functools

import jax
import jax.numpy as jnp
from jax import lax
from jax.experimental import pallas as pl
from jax.experimental.pallas import tpu as pltpu
from jax.sharding import PartitionSpec as P

MESH = pl.DeviceIdType.MESH


def grid_of(n):
    ny = 2
    while ny * ny * 4 <= n:
        ny *= 2
    return n // ny, ny


def fs_of(place, n):
    nz, ny = grid_of(n)
    on = lax.div(place + (n - ny), n)
    rest = (place - ny) * on
    y, r = lax.div(rest, nz - 1), lax.rem(rest, nz - 1)
    odd = lax.rem(y, 2)
    z = 1 + (1 - odd) * r + odd * (nz - 2 - r)
    return on * (z * ny + y) + (1 - on) * (ny - 1 - place)


def place_of(fs, n):
    nz, ny = grid_of(n)
    z, y = lax.div(fs, ny), lax.rem(fs, ny)
    on = lax.div(z + nz - 1, nz)
    up = (z - 1) * on
    odd = lax.rem(y, 2)
    r = (1 - odd) * up + odd * (nz - 2 - up)
    return on * (ny + y * (nz - 1) + r) + (1 - on) * (ny - 1 - y)


def dot(a, b):
    return jnp.dot(a, b, preferred_element_type=jnp.float32)


def kernel(n, n_tp, tokens, gain, gw, uw, dw, out, normed, gacc, uacc, hidden, gbuf, ubuf, dbuf, terms, got,
           send, recv, rs_send, rs_recv, local):
    me, mine = lax.axis_index("fs"), lax.axis_index("tp")
    at = place_of(me, n)
    neighbour = [fs_of(lax.rem(at + 1, n), n), fs_of(lax.rem(at + n - 1, n), n)]
    wide = dw.shape[1]
    rows = gw.shape[0]
    keep = out.shape[0]
    count = normed.shape[0]
    tile = 256

    def owner(way, step):
        step = step if way == 0 else n - step
        return fs_of(lax.rem(at + n - step, n), n)

    barrier = pltpu.get_barrier_semaphore()
    for way in range(2):
        pl.semaphore_signal(barrier, inc=1, device_id={"fs": neighbour[way]}, device_id_type=MESH)
    peers = [lax.rem(mine + k, n_tp) for k in range(1, n_tp)]
    for peer in peers:
        pl.semaphore_signal(barrier, inc=1, device_id={"tp": peer}, device_id_type=MESH)

    loads = [
        pltpu.make_async_copy(tokens, normed, local.at[0]),
        pltpu.make_async_copy(gw, gbuf.at[me], local.at[1]),
        pltpu.make_async_copy(uw, ubuf.at[me], local.at[2]),
        pltpu.make_async_copy(dw, dbuf.at[me], local.at[3]),
    ]
    for load in loads:
        load.start()
    pl.semaphore_wait(barrier, 2 + n_tp - 1)

    def hop(way, own, buf, step, c, event):
        half = own.shape[0] // 2
        part = pl.ds(c * half, half)
        o = owner(way, step)
        return pltpu.make_async_remote_copy(
            src_ref=own.at[part] if step == 0 else buf.at[o, part],
            dst_ref=buf.at[o, part],
            send_sem=send.at[way, event],
            recv_sem=recv.at[way, event],
            device_id={"fs": neighbour[way]},
            device_id_type=MESH,
        )

    def arrive(way, buf, step, c, event):
        half = buf.shape[1] // 2
        here = buf.at[owner(way, step), pl.ds(c * half, half)]
        pltpu.make_async_remote_copy(
            src_ref=here, dst_ref=here, send_sem=send.at[way, event], recv_sem=recv.at[way, event],
            device_id={"fs": neighbour[way]}, device_id_type=MESH,
        ).wait_recv()

    sends = []

    def go(copy):
        copy.start()
        sends.append(copy)

    first = [(gw, gbuf), (uw, ubuf)]
    for c in range(2):
        for way, (own, buf) in enumerate(first):
            go(hop(way, own, buf, 0, c, c))

    loads[0].wait()
    fine = 32

    @pl.loop(0, count // fine)
    def _(i):
        part = pl.ds(pl.multiple_of(i * fine, fine), fine)
        xf = normed[part, :].astype(jnp.float32)
        scale = lax.rsqrt(jnp.mean(xf * xf, axis=-1, keepdims=True) + 1e-06)
        normed[part, :] = (xf * scale * gain[...]).astype(jnp.bfloat16)

    loads[1].wait()
    loads[2].wait()

    def accumulate(step):
        og, ou = owner(0, step), owner(1, step)

        @pl.loop(0, count // tile)
        def _(i):
            part = pl.ds(pl.multiple_of(i * tile, tile), tile)
            for o, buf, acc in ((og, gbuf, gacc), (ou, ubuf, uacc)):
                a = normed[part, pl.ds(pl.multiple_of(o * rows, rows), rows)]
                if step == 0:
                    acc[part, :] = dot(a, buf[o])
                else:
                    acc[part, :] += dot(a, buf[o])

    base = 2 * (n - 1)
    for step in range(1, n):
        for c in range(2):
            for way, (own, buf) in enumerate(first):
                arrive(way, buf, step, c, 2 * (step - 1) + c)
                if step < n - 1:
                    go(hop(way, own, buf, step, c, 2 * step + c))
            if c == 0:
                accumulate(step - 1)
        if step == n - 2:
            for c in range(2):
                for way in range(2):
                    go(hop(way, dw, dbuf, 0, c, base + c))
    accumulate(n - 1)

    @pl.loop(0, count // fine)
    def _(i):
        part = pl.ds(pl.multiple_of(i * fine, fine), fine)
        v = gacc[part, :]
        hidden[part, :] = (v / (1.0 + jnp.exp(-v)) * uacc[part, :]).astype(jnp.bfloat16)

    loads[3].wait()
    shared = []

    def share(o):
        @pl.loop(0, count // tile)
        def _(i):
            part = pl.ds(pl.multiple_of(i * tile, tile), tile)
            terms[o, part, :] = dot(hidden[part, :], dbuf[o]).astype(jnp.bfloat16)

        copies = []
        for k, peer in enumerate(peers):
            copy = pltpu.make_async_remote_copy(
                src_ref=terms.at[o, pl.ds(pl.multiple_of(peer * keep, keep), keep)],
                dst_ref=got.at[k, o],
                send_sem=rs_send.at[len(shared), k],
                recv_sem=rs_recv.at[len(shared), k],
                device_id={"tp": peer},
                device_id_type=MESH,
            )
            go(copy)
            copies.append(copy)
        shared.append((o, copies))

    last = n // 2 - 1
    for step in range(1, n // 2):
        for c in range(2):
            for way in range(2):
                arrive(way, dbuf, step, c, base + 2 * (step - 1) + c)
                if step < last:
                    go(hop(way, dw, dbuf, step, c, base + 2 * step + c))
                elif c == way:
                    go(hop(way, dw, dbuf, step, c, base + 2 * last))
            if step == 1 and c == 0:
                share(me)
        share(owner(0, step))
        share(owner(1, step))
    for way in range(2):
        arrive(way, dbuf, n // 2, way, base + 2 * last)
    share(owner(0, n // 2))

    for o, copies in shared:
        for copy in copies:
            copy.wait_recv()
        total = terms[o, pl.ds(pl.multiple_of(mine * keep, keep), keep), :].astype(jnp.float32)
        for k in range(n_tp - 1):
            total = total + got[k, o].astype(jnp.float32)
        out[:, pl.ds(pl.multiple_of(o * wide, wide), wide)] = total.astype(out.dtype)
    for copy in sends:
        copy.wait_send()


def make_per_device(n, n_tp):
    def per_device(tokens, norm_gain, gate_weight, up_weight, down_weight):
        count, width = tokens.shape
        units = gate_weight.shape[1]
        wide = down_weight.shape[1]
        keep = count // n_tp
        bf16, f32 = jnp.bfloat16, jnp.float32
        events = 2 * (n - 1) + 2 * (n // 2 - 1) + 1
        flops = 6 * count * width * units
        any_ref = pl.BlockSpec(memory_space=pl.ANY)
        vmem_ref = pl.BlockSpec(memory_space=pltpu.VMEM)
        return pl.pallas_call(
            functools.partial(kernel, n, n_tp),
            out_shape=jax.ShapeDtypeStruct((keep, width), bf16),
            in_specs=[any_ref, vmem_ref, any_ref, any_ref, any_ref],
            out_specs=vmem_ref,
            scratch_shapes=[
                pltpu.VMEM((count, width), bf16),
                pltpu.VMEM((count, units), f32),
                pltpu.VMEM((count, units), f32),
                pltpu.VMEM((count, units), bf16),
                pltpu.VMEM((n,) + gate_weight.shape, bf16),
                pltpu.VMEM((n,) + up_weight.shape, bf16),
                pltpu.VMEM((n,) + down_weight.shape, bf16),
                pltpu.VMEM((n, count, wide), bf16),
                pltpu.VMEM((n_tp - 1, n, keep, wide), bf16),
                pltpu.SemaphoreType.DMA((2, events)),
                pltpu.SemaphoreType.DMA((2, events)),
                pltpu.SemaphoreType.DMA((n, n_tp - 1)),
                pltpu.SemaphoreType.DMA((n, n_tp - 1)),
                pltpu.SemaphoreType.DMA((4,)),
            ],
            compiler_params=pltpu.CompilerParams(
                collective_id=0, has_side_effects=True, vmem_limit_bytes=66_000_000
            ),
            cost_estimate=pl.CostEstimate(flops=flops, bytes_accessed=2 * count * width, transcendentals=count * units),
        )(tokens, norm_gain.reshape(1, width), gate_weight, up_weight, down_weight)

    return per_device


def solution(mesh):
    placed = (P("fs", None), P(), P("fs", "tp"), P("fs", "tp"), P("tp", "fs"))
    return jax.shard_map(
        make_per_device(mesh.shape["fs"], mesh.shape["tp"]),
        mesh=mesh, in_specs=placed, out_specs=P(("fs", "tp"), None), check_vma=False,
    )
```

time: 361 us -> 184 us (0.51)
  waiting for transfers between devices: 312 us -> 0 us
  Pallas kernels: 0 us -> 181 us
  matrix products: 32.7 us -> 0 us
  between operations: 13.1 us -> 0.01 us
    all_gather x3 -> x0, waiting for transfers between devices: 267 us -> none  [the longest x1 93.4 us: per_device(): lax.all_gather(down_weight, 'fs', axis=1, tiled=True)]
    pallas_call x0 -> x1, Pallas kernels: none -> 181 us  [per_device(): pl.pallas_call(functools.partial(kernel, n, n_tp), out_shape=jax.ShapeDty...]
    reduce_scatter x1 -> x0, waiting for transfers between devices: 42.9 us -> none  [per_device(): lax.psum_scatter(terms.astype(jnp.bfloat16), 'tp', scatter_dimension=0, t...]
    dot_general x2 -> x0, matrix products: 32.7 us -> none  [the longest x1 20.9 us: per_device(): jnp.dot(hidden, lax.all_gather(down_weight, 'fs', axis=1, tiled=True), pr...]
  transfers between devices with their start and end apart: 4 -> 0, of which waited for: 4 -> 0; matrix products, arithmetic and copies ran while one was open for 4% -> 0% of each run, Pallas kernels for 0% -> 0%
where the time goes in v1:
time: 184 us
  Pallas kernels  181 us (98%)
  local copies, waits for them, and re-layouts  2.3 us (1%)
    pallas_call x1, Pallas kernels, per_device(): pl.pallas_call(functools.partial(kernel, n, n_tp), out_shape=jax.ShapeDty...  181 us

profile of v1, /device:TPU:0, one launch (start us, length us, event | category | flops | bytes accessed | tf_op | source)
XLA Modules:
  0.0 183.6 jit_solution(15458421286429894710)
XLA Ops:
  0.0 181.3 %shard_map.55 = bf16[256,2048]{1,0:T(8,128)(2,1)} custom-call(bf16[1024,2048]{1,0:T(8,128)(2,1)} %tokens.1, f32[1,2048]{1,0:T(1,128)} %bitcast.1, bf16[256,1408]{1,0:T(8,128)(2,1)} %gw.1, bf16[256,1408]{1,0:T(8,128)(2,1)} %uw.1, bf16[1408,256]{1,0:T(8,128)(2,1)} %dw.1), custom_call_target="tpu_custom_call" | custom-call | flops 17716740096 | bytes 4194304 | tf_op jit(solution)/shard_map/pallas_call | solution.py:217
  181.3 2.3 %copy.7 = bf16[256,2048]{1,0:T(8,128)(2,1)} copy(bf16[256,2048]{1,0:T(8,128)(2,1)} %shard_map.55) | data formatting | bytes 2097152

commit v2 on v1

--- a/solution.py
+++ b/solution.py
@@ -41,8 +41,8 @@
     return jnp.dot(a, b, preferred_element_type=jnp.float32)
 
 
-def kernel(n, n_tp, tokens, gain, gw, uw, dw, out, normed, gacc, uacc, hidden, gbuf, ubuf, dbuf, terms, got,
-           send, recv, rs_send, rs_recv, local):
+def kernel(n, n_tp, tokens, gain, gw, uw, dw, out, normed, gacc, uacc, hidden, gbuf, ubuf, dbuf, terms, paired, summed,
+           got, send, recv, pair_send, pair_recv, rs_send, rs_recv, local):
     me, mine = lax.axis_index("fs"), lax.axis_index("tp")
     at = place_of(me, n)
     neighbour = [fs_of(lax.rem(at + 1, n), n), fs_of(lax.rem(at + n - 1, n), n)]
@@ -59,8 +59,11 @@
     barrier = pltpu.get_barrier_semaphore()
     for way in range(2):
         pl.semaphore_signal(barrier, inc=1, device_id={"fs": neighbour[way]}, device_id_type=MESH)
-    peers = [lax.rem(mine + k, n_tp) for k in range(1, n_tp)]
-    for peer in peers:
+    chips = n_tp // 2
+    core, chip = lax.rem(mine, 2), lax.div(mine, 2)
+    partner = 2 * chip + 1 - core
+    others = [lax.rem(chip + k, chips) for k in range(1, chips)]
+    for peer in [partner] + [2 * other + core for other in others]:
         pl.semaphore_signal(barrier, inc=1, device_id={"tp": peer}, device_id_type=MESH)
 
     loads = [
@@ -71,7 +74,7 @@
     ]
     for load in loads:
         load.start()
-    pl.semaphore_wait(barrier, 2 + n_tp - 1)
+    pl.semaphore_wait(barrier, 2 + chips)
 
     def hop(way, own, buf, step, c, event):
         half = own.shape[0] // 2
@@ -155,6 +158,9 @@
     loads[3].wait()
     shared = []
 
+    def kept(index):
+        return pl.ds(pl.multiple_of(index * keep, keep), keep)
+
     def share(o):
         @pl.loop(0, count // tile)
         def _(i):
@@ -162,18 +168,38 @@
             terms[o, part, :] = dot(hidden[part, :], dbuf[o]).astype(jnp.bfloat16)
 
         copies = []
-        for k, peer in enumerate(peers):
+        for k in range(chips):
+            to = lax.rem(chip + 1 + k, chips)
             copy = pltpu.make_async_remote_copy(
-                src_ref=terms.at[o, pl.ds(pl.multiple_of(peer * keep, keep), keep)],
-                dst_ref=got.at[k, o],
-                send_sem=rs_send.at[len(shared), k],
-                recv_sem=rs_recv.at[len(shared), k],
-                device_id={"tp": peer},
+                src_ref=terms.at[o, kept(2 * to + 1 - core)],
+                dst_ref=paired.at[o, k],
+                send_sem=pair_send.at[len(shared), k],
+                recv_sem=pair_recv.at[len(shared), k],
+                device_id={"tp": partner},
                 device_id_type=MESH,
             )
             go(copy)
             copies.append(copy)
-        shared.append((o, copies))
+        shared.append([o, copies, None])
+
+    def cross(j):
+        o, pairs, unused = shared[j]
+        copies = []
+        for k, other in enumerate(others):
+            pairs[k].wait_recv()
+            total = terms[o, kept(2 * other + core), :].astype(jnp.float32) + paired[o, k].astype(jnp.float32)
+            summed[o, k] = total.astype(jnp.bfloat16)
+            copy = pltpu.make_async_remote_copy(
+                src_ref=summed.at[o, k],
+                dst_ref=got.at[k, o],
+                send_sem=rs_send.at[j, k],
+                recv_sem=rs_recv.at[j, k],
+                device_id={"tp": 2 * other + core},
+                device_id_type=MESH,
+            )
+            go(copy)
+            copies.append(copy)
+        shared[j][2] = copies
 
     last = n // 2 - 1
     for step in range(1, n // 2):
@@ -186,17 +212,22 @@
                     go(hop(way, dw, dbuf, step, c, base + 2 * last))
             if step == 1 and c == 0:
                 share(me)
+                cross(0)
         share(owner(0, step))
         share(owner(1, step))
+        cross(2 * step - 1)
+        cross(2 * step)
     for way in range(2):
         arrive(way, dbuf, n // 2, way, base + 2 * last)
     share(owner(0, n // 2))
-
-    for o, copies in shared:
+    cross(n - 1)
+
+    for o, pairs, copies in shared:
+        pairs[chips - 1].wait_recv()
         for copy in copies:
             copy.wait_recv()
-        total = terms[o, pl.ds(pl.multiple_of(mine * keep, keep), keep), :].astype(jnp.float32)
-        for k in range(n_tp - 1):
+        total = terms[o, kept(mine), :].astype(jnp.float32) + paired[o, chips - 1].astype(jnp.float32)
+        for k in range(chips - 1):
             total = total + got[k, o].astype(jnp.float32)
         out[:, pl.ds(pl.multiple_of(o * wide, wide), wide)] = total.astype(out.dtype)
     for copy in sends:
@@ -228,11 +259,15 @@
                 pltpu.VMEM((n,) + up_weight.shape, bf16),
                 pltpu.VMEM((n,) + down_weight.shape, bf16),
                 pltpu.VMEM((n, count, wide), bf16),
-                pltpu.VMEM((n_tp - 1, n, keep, wide), bf16),
+                pltpu.VMEM((n, n_tp // 2, keep, wide), bf16),
+                pltpu.VMEM((n, n_tp // 2 - 1, keep, wide), bf16),
+                pltpu.VMEM((n_tp // 2 - 1, n, keep, wide), bf16),
                 pltpu.SemaphoreType.DMA((2, events)),
                 pltpu.SemaphoreType.DMA((2, events)),
-                pltpu.SemaphoreType.DMA((n, n_tp - 1)),
-                pltpu.SemaphoreType.DMA((n, n_tp - 1)),
+                pltpu.SemaphoreType.DMA((n, n_tp // 2)),
+                pltpu.SemaphoreType.DMA((n, n_tp // 2)),
+                pltpu.SemaphoreType.DMA((n, n_tp // 2 - 1)),
+                pltpu.SemaphoreType.DMA((n, n_tp // 2 - 1)),
                 pltpu.SemaphoreType.DMA((4,)),
             ],
             compiler_params=pltpu.CompilerParams(

time: 184 us -> 181 us (0.984)
  Pallas kernels: 181 us -> 179 us
    pallas_call x1, Pallas kernels: 181 us -> 179 us  [per_device(): pl.pallas_call(functools.partial(kernel, n, n_tp), out_shape=jax.ShapeDty...]
where the time goes in v2:
time: 181 us
  Pallas kernels  179 us (99%)
  local copies, waits for them, and re-layouts  2.3 us (1%)
    pallas_call x1, Pallas kernels, per_device(): pl.pallas_call(functools.partial(kernel, n, n_tp), out_shape=jax.ShapeDty...  179 us

profile of v2, /device:TPU:0, one launch (start us, length us, event | category | flops | bytes accessed | tf_op | source)
XLA Modules:
  0.0 180.9 jit_solution(4889410952583740177)
XLA Ops:
  0.0 178.6 %shard_map.55 = bf16[256,2048]{1,0:T(8,128)(2,1)} custom-call(bf16[1024,2048]{1,0:T(8,128)(2,1)} %tokens.1, f32[1,2048]{1,0:T(1,128)} %bitcast.1, bf16[256,1408]{1,0:T(8,128)(2,1)} %gw.1, bf16[256,1408]{1,0:T(8,128)(2,1)} %uw.1, bf16[1408,256]{1,0:T(8,128)(2,1)} %dw.1), custom_call_target="tpu_custom_call" | custom-call | flops 17716740096 | bytes 4194304 | tf_op jit(solution)/shard_map/pallas_call | solution.py:248
  178.6 2.3 %copy.7 = bf16[256,2048]{1,0:T(8,128)(2,1)} copy(bf16[256,2048]{1,0:T(8,128)(2,1)} %shard_map.55) | data formatting | bytes 2097152

commit v3 on v2

--- a/solution.py
+++ b/solution.py
@@ -35,6 +35,10 @@
     odd = lax.rem(y, 2)
     r = (1 - odd) * up + odd * (nz - 2 - up)
     return on * (ny + y * (nz - 1) + r) + (1 - on) * (ny - 1 - y)
+
+
+def splits_of(wide):
+    return 2 if wide % 256 == 0 else 1
 
 
 def dot(a, b):
@@ -76,22 +80,23 @@
         load.start()
     pl.semaphore_wait(barrier, 2 + chips)
 
-    def hop(way, own, buf, step, c, event):
+    def hop(way, own, buf, step, c, event, cols=None):
         half = own.shape[0] // 2
-        part = pl.ds(c * half, half)
+        part = (pl.ds(c * half, half),) + (() if cols is None else (cols,))
         o = owner(way, step)
         return pltpu.make_async_remote_copy(
-            src_ref=own.at[part] if step == 0 else buf.at[o, part],
-            dst_ref=buf.at[o, part],
+            src_ref=own.at[part] if step == 0 else buf.at[(o,) + part],
+            dst_ref=buf.at[(o,) + part],
             send_sem=send.at[way, event],
             recv_sem=recv.at[way, event],
             device_id={"fs": neighbour[way]},
             device_id_type=MESH,
         )
 
-    def arrive(way, buf, step, c, event):
+    def arrive(way, buf, step, c, event, cols=None):
         half = buf.shape[1] // 2
-        here = buf.at[owner(way, step), pl.ds(c * half, half)]
+        part = (pl.ds(c * half, half),) + (() if cols is None else (cols,))
+        here = buf.at[(owner(way, step),) + part]
         pltpu.make_async_remote_copy(
             src_ref=here, dst_ref=here, send_sem=send.at[way, event], recv_sem=recv.at[way, event],
             device_id={"fs": neighbour[way]}, device_id_type=MESH,
@@ -157,22 +162,25 @@
 
     loads[3].wait()
     shared = []
+    whole = pl.ds(0, wide)
+    cuts = splits_of(wide)
+    narrow = [pl.ds(v * (wide // cuts), wide // cuts) for v in range(cuts)]
 
     def kept(index):
         return pl.ds(pl.multiple_of(index * keep, keep), keep)
 
-    def share(o):
+    def share(o, cols=whole):
         @pl.loop(0, count // tile)
         def _(i):
             part = pl.ds(pl.multiple_of(i * tile, tile), tile)
-            terms[o, part, :] = dot(hidden[part, :], dbuf[o]).astype(jnp.bfloat16)
+            terms[o, part, cols] = dot(hidden[part, :], dbuf[o, :, cols]).astype(jnp.bfloat16)
 
         copies = []
         for k in range(chips):
             to = lax.rem(chip + 1 + k, chips)
             copy = pltpu.make_async_remote_copy(
-                src_ref=terms.at[o, kept(2 * to + 1 - core)],
-                dst_ref=paired.at[o, k],
+                src_ref=terms.at[o, kept(2 * to + 1 - core), cols],
+                dst_ref=paired.at[o, k, :, cols],
                 send_sem=pair_send.at[len(shared), k],
                 recv_sem=pair_recv.at[len(shared), k],
                 device_id={"tp": partner},
@@ -180,18 +188,18 @@
             )
             go(copy)
             copies.append(copy)
-        shared.append([o, copies, None])
+        shared.append([o, copies, None, cols])
 
     def cross(j):
-        o, pairs, unused = shared[j]
+        o, pairs, unused, cols = shared[j]
         copies = []
         for k, other in enumerate(others):
             pairs[k].wait_recv()
-            total = terms[o, kept(2 * other + core), :].astype(jnp.float32) + paired[o, k].astype(jnp.float32)
-            summed[o, k] = total.astype(jnp.bfloat16)
+            total = terms[o, kept(2 * other + core), cols].astype(jnp.float32) + paired[o, k, :, cols].astype(jnp.float32)
+            summed[o, k, :, cols] = total.astype(jnp.bfloat16)
             copy = pltpu.make_async_remote_copy(
-                src_ref=summed.at[o, k],
-                dst_ref=got.at[k, o],
+                src_ref=summed.at[o, k, :, cols],
+                dst_ref=got.at[k, o, :, cols],
                 send_sem=rs_send.at[j, k],
                 recv_sem=rs_recv.at[j, k],
                 device_id={"tp": 2 * other + core},
@@ -209,7 +217,8 @@
                 if step < last:
                     go(hop(way, dw, dbuf, step, c, base + 2 * step + c))
                 elif c == way:
-                    go(hop(way, dw, dbuf, step, c, base + 2 * last))
+                    for v, cols in enumerate(narrow):
+                        go(hop(way, dw, dbuf, step, c, base + 2 * last + v, cols))
             if step == 1 and c == 0:
                 share(me)
                 cross(0)
@@ -217,19 +226,20 @@
         share(owner(1, step))
         cross(2 * step - 1)
         cross(2 * step)
-    for way in range(2):
-        arrive(way, dbuf, n // 2, way, base + 2 * last)
-    share(owner(0, n // 2))
-    cross(n - 1)
-
-    for o, pairs, copies in shared:
+    for v, cols in enumerate(narrow):
+        for way in range(2):
+            arrive(way, dbuf, n // 2, way, base + 2 * last + v, cols)
+        share(owner(0, n // 2), cols)
+        cross(n - 1 + v)
+
+    for o, pairs, copies, cols in shared:
         pairs[chips - 1].wait_recv()
         for copy in copies:
             copy.wait_recv()
-        total = terms[o, kept(mine), :].astype(jnp.float32) + paired[o, chips - 1].astype(jnp.float32)
+        total = terms[o, kept(mine), cols].astype(jnp.float32) + paired[o, chips - 1, :, cols].astype(jnp.float32)
         for k in range(chips - 1):
-            total = total + got[k, o].astype(jnp.float32)
-        out[:, pl.ds(pl.multiple_of(o * wide, wide), wide)] = total.astype(out.dtype)
+            total = total + got[k, o, :, cols].astype(jnp.float32)
+        out[:, pl.ds(pl.multiple_of(o * wide + cols.start, cols.size), cols.size)] = total.astype(out.dtype)
     for copy in sends:
         copy.wait_send()
 
@@ -241,7 +251,8 @@
         wide = down_weight.shape[1]
         keep = count // n_tp
         bf16, f32 = jnp.bfloat16, jnp.float32
-        events = 2 * (n - 1) + 2 * (n // 2 - 1) + 1
+        cuts = splits_of(wide)
+        events = 2 * (n - 1) + 2 * (n // 2 - 1) + cuts
         flops = 6 * count * width * units
         any_ref = pl.BlockSpec(memory_space=pl.ANY)
         vmem_ref = pl.BlockSpec(memory_space=pltpu.VMEM)
@@ -264,10 +275,10 @@
                 pltpu.VMEM((n_tp // 2 - 1, n, keep, wide), bf16),
                 pltpu.SemaphoreType.DMA((2, events)),
                 pltpu.SemaphoreType.DMA((2, events)),
-                pltpu.SemaphoreType.DMA((n, n_tp // 2)),
-                pltpu.SemaphoreType.DMA((n, n_tp // 2)),
-                pltpu.SemaphoreType.DMA((n, n_tp // 2 - 1)),
-                pltpu.SemaphoreType.DMA((n, n_tp // 2 - 1)),
+                pltpu.SemaphoreType.DMA((n - 1 + cuts, n_tp // 2)),
+                pltpu.SemaphoreType.DMA((n - 1 + cuts, n_tp // 2)),
+                pltpu.SemaphoreType.DMA((n - 1 + cuts, n_tp // 2 - 1)),
+                pltpu.SemaphoreType.DMA((n - 1 + cuts, n_tp // 2 - 1)),
                 pltpu.SemaphoreType.DMA((4,)),
             ],
             compiler_params=pltpu.CompilerParams(

time: 181 us -> 181 us (level)
  no operation moved by 1% of the time
where the time goes in v3:
time: 181 us
  Pallas kernels  178 us (98%)
  local copies, waits for them, and re-layouts  2.3 us (1%)
    pallas_call x1, Pallas kernels, per_device(): pl.pallas_call(functools.partial(kernel, n, n_tp), out_shape=jax.ShapeDty...  178 us

profile of v3, /device:TPU:0, one launch (start us, length us, event | category | flops | bytes accessed | tf_op | source)
XLA Modules:
  0.0 180.7 jit_solution(11998009748128546185)
XLA Ops:
  0.0 178.4 %shard_map.55 = bf16[256,2048]{1,0:T(8,128)(2,1)} custom-call(bf16[1024,2048]{1,0:T(8,128)(2,1)} %tokens.1, f32[1,2048]{1,0:T(1,128)} %bitcast.1, bf16[256,1408]{1,0:T(8,128)(2,1)} %gw.1, bf16[256,1408]{1,0:T(8,128)(2,1)} %uw.1, bf16[1408,256]{1,0:T(8,128)(2,1)} %dw.1), custom_call_target="tpu_custom_call" | custom-call | flops 17716740096 | bytes 4194304 | tf_op jit(solution)/shard_map/pallas_call | solution.py:259
  178.4 2.3 %copy.7 = bf16[256,2048]{1,0:T(8,128)(2,1)} copy(bf16[256,2048]{1,0:T(8,128)(2,1)} %shard_map.55) | data formatting | bytes 2097152

commit v4 on v3

--- a/solution.py
+++ b/solution.py
@@ -151,7 +151,7 @@
         if step == n - 2:
             for c in range(2):
                 for way in range(2):
-                    go(hop(way, dw, dbuf, 0, c, base + c))
+                    go(hop(way, dw, dbuf, 0, c ^ way, base + c))
     accumulate(n - 1)
 
     @pl.loop(0, count // fine)
@@ -213,12 +213,12 @@
     for step in range(1, n // 2):
         for c in range(2):
             for way in range(2):
-                arrive(way, dbuf, step, c, base + 2 * (step - 1) + c)
+                arrive(way, dbuf, step, c ^ way, base + 2 * (step - 1) + c)
                 if step < last:
-                    go(hop(way, dw, dbuf, step, c, base + 2 * step + c))
-                elif c == way:
+                    go(hop(way, dw, dbuf, step, c ^ way, base + 2 * step + c))
+                elif c == 0:
                     for v, cols in enumerate(narrow):
-                        go(hop(way, dw, dbuf, step, c, base + 2 * last + v, cols))
+                        go(hop(way, dw, dbuf, step, way, base + 2 * last + v, cols))
             if step == 1 and c == 0:
                 share(me)
                 cross(0)

time: 181 us -> 180 us (level)
  no operation moved by 1% of the time
where the time goes in v4:
time: 180 us
  Pallas kernels  178 us (99%)
  local copies, waits for them, and re-layouts  2.3 us (1%)
    pallas_call x1, Pallas kernels, per_device(): pl.pallas_call(functools.partial(kernel, n, n_tp), out_shape=jax.ShapeDty...  178 us

profile of v4, /device:TPU:0, one launch (start us, length us, event | category | flops | bytes accessed | tf_op | source)
XLA Modules:
  0.0 179.9 jit_solution(9961788151950472168)
XLA Ops:
  0.0 177.6 %shard_map.55 = bf16[256,2048]{1,0:T(8,128)(2,1)} custom-call(bf16[1024,2048]{1,0:T(8,128)(2,1)} %tokens.1, f32[1,2048]{1,0:T(1,128)} %bitcast.1, bf16[256,1408]{1,0:T(8,128)(2,1)} %gw.1, bf16[256,1408]{1,0:T(8,128)(2,1)} %uw.1, bf16[1408,256]{1,0:T(8,128)(2,1)} %dw.1), custom_call_target="tpu_custom_call" | custom-call | flops 17716740096 | bytes 4194304 | tf_op jit(solution)/shard_map/pallas_call | solution.py:259
  177.6 2.3 %copy.7 = bf16[256,2048]{1,0:T(8,128)(2,1)} copy(bf16[256,2048]{1,0:T(8,128)(2,1)} %shard_map.55) | data formatting | bytes 2097152
